TPU v7x, 256 devices: a whole 4x4x8 slice. The times are simulated.
256 devices in a mesh: sp: 64 (over z, y, core), tp: 4 (over x).
Axes of the slice: x: 4, y: 4, z: 8, core: 2. Of those that a mesh axis runs over, the one named last changes fastest.
Arguments:
- stream_in: bfloat16 [49152, 2048], P(('sp', 'tp')), may hold values from -6 to 6
- query_wide: bfloat16 [49152, 512], P('sp', 'tp'), may hold values from -6 to 6
- key_wide: bfloat16 [49152, 512], P('sp', 'tp'), may hold values from -6 to 6
- value_wide: bfloat16 [49152, 512], P('sp', 'tp'), may hold values from -6 to 6
- gate_wide: bfloat16 [49152, 512], P('sp', 'tp'), may hold values from -6 to 6
- decay_wide: float32 [4, 49152], P('tp', 'sp'), may hold values from -2.3 to 0, as said below
- query_narrow: bfloat16 [49152, 512], P('sp', 'tp'), may hold values from -6 to 6
- key_narrow: bfloat16 [49152, 512], P('sp', 'tp'), may hold values from -6 to 6
- value_narrow: bfloat16 [49152, 512], P('sp', 'tp'), may hold values from -6 to 6
- gate_narrow: bfloat16 [49152, 512], P('sp', 'tp'), may hold values from -6 to 6
- decay_narrow: float32 [8, 49152], P('tp', 'sp'), may hold values from -2.3 to 0, as said below
- output_wide: bfloat16 [512, 2048], P('tp'), may hold values from -0.25 to 0.25
- output_narrow: bfloat16 [512, 2048], P('tp'), may hold values from -0.25 to 0.25
- norm_gain: bfloat16 [2048], replicated, may hold values from 0.099609375 to 1.8984375
- up_weight: bfloat16 [2048, 8192], P('sp', 'tp'), may hold values from -0.125 to 0.125
- down_weight: bfloat16 [8192, 2048], P('tp', 'sp'), may hold values from -0.0625 to 0.0625
Outputs:
- layer_out: bfloat16 [49152, 2048], P(('sp', 'tp'))
Inputs may be any that keep to these rules, and one draw needn't show every extreme that they name: `decay_wide`: each entry is the logarithm of one head's retention factor at one position. `decay_narrow`: each entry is the logarithm of one head's retention factor at one position.
All inputs are finite; a program needn't handle non-finite values.
Results may differ from a plain program's by a relative error of at most 0.02.
Values may be sent and summed in bfloat16 or wider, within the bound.
A program may use at most 128 MiB of HBM per device.

v0:
```python
import jax
import jax.numpy as jnp
from jax import lax
from jax.sharding import Mesh
from jax.sharding import PartitionSpec as P

HDW = 128
HDN = 64
BLOCK = 128
SP = ("sp_0", "sp_1", "sp_2")
SP_TP = ("sp_0", "sp_1", "sp_2", "tp")
head_eps = 1e-05
norm_eps = 1e-06
rope_base = 10000.0


def rows_first(arrays, axis, dims):
    turned = [jnp.moveaxis(a, dim, 0) for a, dim in zip(arrays, dims)]
    both = jnp.concatenate([t.reshape(len(t), -1) for t in turned], axis=1)
    out, at, finished = (lax.all_gather(both, axis, axis=0, tiled=True), 0, [])
    for t, dim in zip(turned, dims):
        section = out[:, at : at + t[0].size].reshape(-1, *t.shape[1:])
        finished.append(jnp.moveaxis(section, 0, dim))
        at += t[0].size
    return tuple(finished)


def nothing_yet(shard, identity):
    return jax.tree.map(
        lambda part, zero: jnp.zeros_like(part) + jnp.asarray(zero, part.dtype), shard, identity
    )


def gathered_once(shard, axis):
    leaves = jax.tree.leaves(shard)
    sequence = sorted(range(len(leaves)), key=lambda k: -leaves[k].size)
    width = (1, *leaves[sequence[0]].shape)[-1]
    lines = [
        jnp.pad(leaves[k].reshape(-1), (0, -leaves[k].size % width)).reshape(-1, width)
        for k in sequence
    ]
    both, at, found = (lax.all_gather(jnp.concatenate(lines), axis), 0, {})
    for k, line in zip(sequence, lines):
        section = both[:, at : at + len(line)].reshape(len(both), -1)
        found[k] = section[:, : leaves[k].size].reshape(-1, *leaves[k].shape)
        at += len(line)
    numbers = iter(range(len(leaves)))
    return jax.tree.map(lambda _: found[next(numbers)], shard)


def entering(shard, axes, combine, identity):
    before = start = nothing_yet(shard, identity)
    so_far = shard
    for axis in reversed(axes):
        length, mine = (lax.axis_size(axis), lax.axis_index(axis))
        pieces = gathered_once(
            jax.tree.map(
                lambda part, kind: part.astype(kind),
                so_far,
                (jnp.bfloat16, jnp.bfloat16, jnp.bfloat16, jnp.bfloat16),
            ),
            axis,
        )
        inside, so_far = (start, start)
        for k in range(length):
            passed = k < mine
            so_far = combine(
                so_far, jax.tree.map(lambda part, own: part[k].astype(own.dtype), pieces, shard)
            )
            inside = jax.tree.map(lambda new, old: jnp.where(passed, new, old), so_far, inside)
        before = combine(inside, before)
    return before


def in_blocks(shard, dim, length):
    before, after = (shard.shape[:dim], shard.shape[dim + 1 :])
    return jnp.moveaxis(shard.reshape(*before, length, -1, *after), dim, 0)


def sum_at_owner(shard, axis, dim):
    tiles = in_blocks(shard, dim, lax.axis_size(axis))
    arrived = lax.all_to_all(tiles, axis, split_axis=0, concat_axis=0, tiled=True)
    return arrived.astype(jnp.float32).sum(axis=0)


def rotate(values, places):
    half = values.shape[-1] // 2
    inverse = rope_base ** (-jnp.arange(half, dtype=jnp.float32) / half)
    angles = places[:, None] * inverse[None, :]
    cosine = jnp.cos(angles)[:, None, :]
    sine = jnp.sin(angles)[:, None, :]
    front = values[..., :half]
    back = values[..., half:]
    return jnp.concatenate([front * cosine - back * sine, back * cosine + front * sine], axis=-1)


def block_step(carried, inputs):
    query, keys, values, log_rate = inputs
    running = jnp.cumsum(log_rate, axis=0)
    spread = running[:, None, :] - running[None, :, :]
    length = log_rate.shape[0]
    lower = (jnp.arange(length)[:, None] >= jnp.arange(length)[None, :])[:, :, None]
    factor = jnp.where(lower, jnp.exp(jnp.minimum(spread, 0.0)), 0.0)
    scores = jnp.einsum("thd,shd->tsh", query, keys) * factor
    within = jnp.einsum("tsh,she->the", scores, values)
    across = jnp.einsum("thd,hde->the", query, carried) * jnp.exp(running)[:, :, None]
    tail_decay = jnp.exp(running[-1][None, :] - running)
    updated = jnp.exp(running[-1])[:, None, None] * carried + jnp.einsum(
        "shd,she->hde", keys * tail_decay[:, :, None], values
    )
    return (updated, within + across)


def head_norm(values):
    centre = values - jnp.mean(values, axis=-1, keepdims=True)
    spread = jnp.mean(centre * centre, axis=-1, keepdims=True)
    return centre * lax.rsqrt(spread + head_eps)


def local_group(query, keys, values, log_rate, width, places):
    length = query.shape[0]
    count_of_heads = query.shape[1] // width
    blocks = length // BLOCK

    def split(array):
        return array.astype(jnp.float32).reshape(length, count_of_heads, width)

    query_rot = rotate(split(query), places)
    keys_rot = rotate(split(keys), places) * width ** (-0.5)
    rates = log_rate.T
    carried = jnp.zeros((count_of_heads, width, width), jnp.float32)
    final_state, outputs = lax.scan(
        block_step,
        carried,
        (
            query_rot.reshape(blocks, BLOCK, count_of_heads, width),
            keys_rot.reshape(blocks, BLOCK, count_of_heads, width),
            split(values).reshape(blocks, BLOCK, count_of_heads, width),
            rates.reshape(blocks, BLOCK, count_of_heads),
        ),
    )
    running = jnp.cumsum(rates, axis=0)
    return (
        query_rot,
        outputs.reshape(length, count_of_heads, width),
        final_state,
        jnp.exp(running[-1]),
        running,
    )


def finish_group(query_rot, outputs, incoming, running, gate):
    length = outputs.shape[0]
    outputs = (
        outputs + jnp.einsum("thd,hde->the", query_rot, incoming) * jnp.exp(running)[:, :, None]
    )
    normed = head_norm(outputs).reshape(length, -1)
    return (jax.nn.silu(gate.astype(jnp.float32)) * normed).astype(jnp.bfloat16)


def chain(earlier, later):
    rate_wide, memory_wide, rate_narrow, memory_narrow = earlier
    later_rate_wide, later_memory_wide, later_rate_narrow, later_memory_narrow = later
    return (
        rate_wide * later_rate_wide,
        memory_wide * later_rate_wide[:, None, None] + later_memory_wide,
        rate_narrow * later_rate_narrow,
        memory_narrow * later_rate_narrow[:, None, None] + later_memory_narrow,
    )


def row_norm(middle, norm_gain):
    middle_f = middle.astype(jnp.float32)
    scale = lax.rsqrt(jnp.mean(middle_f * middle_f, axis=-1, keepdims=True) + norm_eps)
    return (middle_f * scale * norm_gain.astype(jnp.float32)).astype(jnp.bfloat16)


def on_device(
    stream_in,
    query_wide,
    key_wide,
    value_wide,
    gate_wide,
    decay_wide,
    query_narrow,
    key_narrow,
    value_narrow,
    gate_narrow,
    decay_narrow,
    output_wide,
    output_narrow,
    norm_gain,
    up_weight,
    down_weight,
):
    length = query_wide.shape[0]
    up_full, down_full = rows_first((up_weight, down_weight), SP, (0, 1))
    places = (lax.axis_index(SP) * length + jnp.arange(length, dtype=jnp.int32)).astype(jnp.float32)
    wide_query, wide_out, wide_state, wide_total, wide_running = local_group(
        query_wide, key_wide, value_wide, decay_wide, HDW, places
    )
    narrow_query, narrow_out, narrow_state, narrow_total, narrow_running = local_group(
        query_narrow, key_narrow, value_narrow, decay_narrow, HDN, places
    )
    identity = (
        jnp.ones_like(wide_total),
        jnp.zeros_like(wide_state),
        jnp.ones_like(narrow_total),
        jnp.zeros_like(narrow_state),
    )
    incoming = entering((wide_total, wide_state, narrow_total, narrow_state), SP, chain, identity)
    mixed_wide = finish_group(wide_query, wide_out, incoming[1], wide_running, gate_wide)
    mixed_narrow = finish_group(narrow_query, narrow_out, incoming[3], narrow_running, gate_narrow)
    mixed_sum = sum_at_owner(
        (
            jnp.dot(mixed_wide, output_wide, preferred_element_type=jnp.float32)
            + jnp.dot(mixed_narrow, output_narrow, preferred_element_type=jnp.float32)
        ).astype(jnp.bfloat16),
        "tp",
        0,
    )
    middle = (stream_in.astype(jnp.float32) + mixed_sum).astype(jnp.bfloat16)
    normed = lax.all_gather(row_norm(middle, norm_gain), "tp", axis=0, tiled=True)
    up_sum = jnp.dot(normed, up_full, preferred_element_type=jnp.float32)
    hidden = jnp.square(jax.nn.relu(up_sum)).astype(jnp.bfloat16)
    down_sum = jnp.dot(hidden, down_full, preferred_element_type=jnp.float32)
    down_rows = lax.psum_scatter(
        down_sum.astype(jnp.bfloat16), "tp", scatter_dimension=0, tiled=True
    ).astype(jnp.float32)
    return (middle.astype(jnp.float32) + down_rows).astype(jnp.bfloat16)


def solution(mesh):
    split = Mesh(mesh.devices.reshape(8, 4, 2, mesh.shape["tp"]), ("sp_0", "sp_1", "sp_2", "tp"))
    in_specs = (
        P(SP_TP, None),
        P(SP, "tp"),
        P(SP, "tp"),
        P(SP, "tp"),
        P(SP, "tp"),
        P("tp", SP),
        P(SP, "tp"),
        P(SP, "tp"),
        P(SP, "tp"),
        P(SP, "tp"),
        P("tp", SP),
        P("tp", None),
        P("tp", None),
        P(),
        P(SP, "tp"),
        P("tp", SP),
    )
    out_specs = P(SP_TP, None)
    return jax.shard_map(
        on_device, mesh=split, in_specs=in_specs, out_specs=out_specs, check_vma=False
    )
```

profile of v0, /device:TPU:1, one launch (start us, length us, event | category | flops | bytes accessed | tf_op | source)
XLA Modules:
  0.0 398.5 jit_solution(7533716243381743910)
XLA Ops:
  6.6 1.1 copy.156
  7.8 1.1 copy.158
  10.4 25.0 %while.27 = (s32[]{:T(128)}, f32[2,64,64]{2,1,0:T(8,128)S(1)}, f32[6,128,2,64]{1,0,3,2:T(8,128)}, f32[6,128,2]{2,1,0:T(8,128)S(1)}, f32[6,128,2,64]{1,0,3,2:T(8,...) while((s32[]{:T(128)}, f32[2,64,64]{2,1,0:T(8,128)S(1)}, ...), condition=%wide.region_5.6_spmd.clone, body=%wide.region_3.5_spmd.clone.sunk | while | flops 12877827 | bytes 1099440 | solution.py:132
  11.5 2.8 dynamic_update_slice.14
  15.7 2.8 dynamic_update_slice.14
  19.9 2.8 dynamic_update_slice.14
  24.0 2.8 dynamic_update_slice.14
  28.2 2.8 dynamic_update_slice.14
  32.3 2.8 dynamic_update_slice.14
  35.5 1.0 reshape_reshape.22
  36.5 1.9 fusion.88
  38.6 0.9 maximum_multiply_fusion.1
  39.5 22.9 %while.26 = (s32[]{:T(128)}, f32[1,128,128]{2,1,0:T(8,128)S(1)}, f32[6,128,1,128]{3,1,0,2:T(8,128)}, f32[6,128,1]{1,2,0:T(1,128)S(1)}, f32[6,128,1,128]{3,2,1,0:...) while((s32[]{:T(128)}, f32[1,128,128]{2,1,0:T(8,128)S(1)}, ...), condition=%wide.region_2.3_spmd.clone, body=%wide.region_0.2_spmd.clone.sunk | while | flops 17006596 | bytes 1515172 | solution.py:132
  67.1 4.7 %all-gather.3 = bf16[2,194,128]{2,1,0:T(8,128)(2,1)S(1)} all-gather(bf16[1,194,128]{2,1,0:T(8,128)(2,1)S(1)} %maximum_bitcast_fusion), channel_id=2, replica_groups=mesh['sp_0'=8,'sp_1'=4,'sp_2'=2,'tp'=4] {'sp_2'}, dimensions={0}, use_global_device_ids=true | all-gather | bytes 148992 | tf_op jit(solution)/shard_map/all_gather | solution.py:42
  74.8 9.3 %all-gather.4 = bf16[4,194,128]{2,1,0:T(8,128)(2,1)S(1)} all-gather(bf16[1,194,128]{2,1,0:T(8,128)(2,1)S(1)} %maximum_bitcast_fusion.1), channel_id=3, replica_groups=mesh['sp_0'=8,'sp_1'=4,'sp_2'=2,'tp'=4] {'sp_1'}, dimensions={0}, use_global_device_ids=true | all-gather | bytes 248320 | tf_op jit(solution)/shard_map/all_gather | solution.py:42
  89.2 21.5 %all-gather.5 = bf16[8,194,128]{2,1,0:T(8,128)(2,1)S(1)} all-gather(bf16[1,194,128]{2,1,0:T(8,128)(2,1)S(1)} %maximum_bitcast_fusion.2), channel_id=4, replica_groups=mesh['sp_0'=8,'sp_1'=4,'sp_2'=2,'tp'=4] {'sp_0'}, dimensions={0}, use_global_device_ids=true | all-gather | bytes 446976 | tf_op jit(solution)/shard_map/all_gather | solution.py:42
  125.4 1.6 fusion.292
  127.1 1.1 copy.170
  134.7 1.2 copy.169
  136.6 1.2 fusion.291
  137.8 1.1 copy.153
  139.1 1.0 fusion.93
  140.1 2.7 add_convert_fusion
  142.8 4.8 %all-to-all-start = ((bf16[4,192,2048]{2,1,0:T(8,128)(2,1)}), bf16[4,192,2048]{2,1,0:T(8,128)(2,1)}, u32[]{:S(2)}, u32[]{:S(2)}) async-start(bf16[4,192,2048]{2,1,0:T(8,128)(2,1)} %bitcast.454), calls=%async_computation | async-start | bytes 6291456 | tf_op jit(solution)/shard_map/all_to_all | solution.py:82
  147.8 27.9 %all-to-all-done = bf16[4,192,2048]{2,1,0:T(8,128)(2,1)} async-done(((bf16[4,192,2048]{2,1,0:T(8,128)(2,1)}), bf16[4,192,2048]{2,1,0:T(8,128)(2,1)}, u32[]{:S(2)}, u32[]{:S(2)}) %all-to-all-start) | async-done | bytes 3145760 | tf_op jit(solution)/shard_map/all_to_all | solution.py:82
  175.8 2.7 convert_reduce_fusion
  178.8 1.1 fusion.63
  180.9 47.7 %all-gather.9.cloned.1.call-done = bf16[768,2048]{1,0:T(8,128)(2,1)} async-done(((bf16[192,2048]{1,0:T(8,128)(2,1)}), bf16[768,2048]{1,0:T(8,128)(2,1)}) %all-gather.9.cloned.1.call-update) | async-done | bytes 3145744 | tf_op jit(solution)/shard_map/all_gather | solution.py:223
  228.6 102.9 %all-gather.11.cloned.1.call-done = bf16[2048,4096]{1,0:T(8,128)(2,1)} async-done(((bf16[32,4096]{1,0:T(8,128)(2,1)}), bf16[2048,4096]{1,0:T(8,128)(2,1)}) %all-gather.11.cloned.1.call-update) | async-done | bytes 16777232 | tf_op jit(solution)/shard_map/all_gather | solution.py:20
  331.5 20.7 %fusion.55 = bf16[768,2048]{1,0:T(8,128)(2,1)} fusion(bf16[2048,4096]{1,0:T(8,128)(2,1)} %all-gather.11.cloned.1.call-done, bf16[768,2048]{1,0:T(8,128)(2,1)} %all-gather.9.cloned.1.call-done), kind=kOutput, calls=%fused_computation.75 | convolution fusion | flops 12891193344 | bytes 23068672 | tf_op jit(solution)/shard_map/dot_general | solution.py:226
  352.2 37.5 %reduce-scatter.2.cloned.1.call-done = bf16[192,2048]{1,0:T(8,128)(2,1)} async-done(((bf16[768,2048]{1,0:T(8,128)(2,1)}), bf16[192,2048]{1,0:T(8,128)(2,1)}) %reduce-scatter.2.cloned.1.call-update) | async-done | bytes 786448 | tf_op jit(solution)/shard_map/reduce_scatter | solution.py:227
  389.7 2.3 fusion.64
  (320 shorter events, 51.5 us)
Async XLA Ops:
  6.5 132.5 %copy-start = (bf16[128,2048]{1,0:T(8,128)(2,1)S(1)}, bf16[128,2048]{1,0:T(8,128)(2,1)}, u32[]{:S(2)}) copy-start(bf16[128,2048]{1,0:T(8,128)(2,1)} %param.31) | copy-start | bytes 1572868
  6.5 3.0 copy-start.6
  7.8 2.3 copy-start.9
  10.4 26.1 %copy-start.4 = (bf16[768,128]{1,0:T(8,128)(2,1)S(1)}, bf16[768,128]{1,0:T(8,128)(2,1)}, u32[]{:S(2)}) copy-start(bf16[768,128]{1,0:T(8,128)(2,1)} %param.21) | copy-start | bytes 589828
  10.4 26.0 %copy-start.5 = (bf16[768,128]{1,0:T(8,128)(2,1)S(1)}, bf16[768,128]{1,0:T(8,128)(2,1)}, u32[]{:S(2)}) copy-start(bf16[768,128]{1,0:T(8,128)(2,1)} %param.22) | copy-start | bytes 589828
  36.5 3.0 copy-start.14
  71.8 15.4 %copy-start.15 = (f32[2]{0:T(128)}, f32[2]{0:T(128)S(1)}, u32[]{:S(2)}) copy-start(f32[2]{0:T(128)S(1)} %bitcast_convert_fusion.12) | copy-start | bytes 28
  73.3 52.0 %copy-start.3 = (f32[6,128,2,64]{1,0,3,2:T(8,128)S(1)}, f32[6,128,2,64]{1,0,3,2:T(8,128)}, u32[]{:S(2)}) copy-start(f32[6,128,2,64]{1,0,3,2:T(8,128)} %get-tuple-element.84) | copy-start | bytes 1179652
  87.2 0.9 copy-start.12
  87.2 1.1 copy-start.11
  87.2 23.5 %copy-start.10 = (f32[2]{0:T(128)}, f32[2]{0:T(128)S(1)}, u32[]{:S(2)}) copy-start(f32[2]{0:T(128)S(1)} %get-tuple-element.255) | copy-start | bytes 28
  139.0 1.1 copy-start.2
  142.8 5.0 %copy-start.13 = (bf16[2048]{0:T(1024)(128)(2,1)S(1)}, bf16[2048]{0:T(1024)(128)(2,1)}, u32[]{:S(2)}) copy-start(bf16[2048]{0:T(1024)(128)(2,1)} %param.33) | copy-start | bytes 12292
  142.8 33.0 %all-to-all-start = ((bf16[4,192,2048]{2,1,0:T(8,128)(2,1)}), bf16[4,192,2048]{2,1,0:T(8,128)(2,1)}, u32[]{:S(2)}, u32[]{:S(2)}) async-start(bf16[4,192,2048]{2,1,0:T(8,128)(2,1)} %bitcast.454), calls=%async_computation | async-start | bytes 6291456 | tf_op jit(solution)/shard_map/all_to_all | solution.py:82
  147.6 30.9 %copy-start.1 = (bf16[192,2048]{1,0:T(8,128)(2,1)S(1)}, bf16[192,2048]{1,0:T(8,128)(2,1)}, u32[]{:S(2)}) copy-start(bf16[192,2048]{1,0:T(8,128)(2,1)} %param.20) | copy-start | bytes 2359300
  147.6 81.0 %all-gather.9.cloned.1.call-start = ((), (), s32[]{:S(2)}) async-start(), calls=%async_computation.2 | async-start | bytes 3932160 | tf_op jit(solution)/shard_map/all_gather | solution.py:223
  178.5 1.6 copy-start.7
  178.5 1.6 copy-start.8
  180.0 151.5 %all-gather.11.cloned.1.call-start = ((), (), s32[]{:S(2)}) async-start(), calls=%async_computation.3 | async-start | bytes 17039360 | tf_op jit(solution)/shard_map/all_gather | solution.py:20
  180.8 208.9 %reduce-scatter.2.cloned.1.call-start = ((), (), s32[]{:S(2)}) async-start(), calls=%async_computation.4 | async-start | bytes 3932160 | tf_op jit(solution)/shard_map/reduce_scatter | solution.py:227
Sparse Core Ops, SparseCore 0:
  180.1 48.4 all-gather.8
  231.4 100.0 all-gather.10
  352.4 37.3 reduce-scatter.1
where the time goes:
time: 400 us; the launch traced here: 399 us
  waiting for transfers between devices  216 us (54%)
  local copies, waits for them, and re-layouts  50.2 us (13%)
  matrix products  35.7 us (9%)
  blocking collectives  35.5 us (9%)
  between operations  26.9 us (7%)
  other arithmetic  24.5 us (6%)
  starting transfers between devices  5.08 us (1%)
  loops' own time  4.6 us (1%)
    all_gather x1, waiting for transfers between devices, rows_first(): out, at, finished = (lax.all_gather(both, axis, axis=0, tiled=True), 0, [])  103 us
    all_gather x1, waiting for transfers between devices, on_device(): lax.all_gather(row_norm(middle, norm_gain), 'tp', axis=0, tiled=True)  47.7 us
    reduce_scatter x1, waiting for transfers between devices, on_device(): lax.psum_scatter(down_sum.astype(jnp.bfloat16), 'tp', scatter_dimension=0...  37.5 us
    all_gather x3, blocking collectives, gathered_once(): both, at, found = (lax.all_gather(jnp.concatenate(lines), axis), 0, {})  35.5 us
    all_to_all x1, waiting for transfers between devices, sum_at_owner(): lax.all_to_all(tiles, axis, split_axis=0, concat_axis=0, tiled=True)  27.9 us
    dynamic_update_slice x18, local copies, waits for them, and re-layouts, local_group(): lax.scan(block_step, carried, (query_rot.reshape(blocks, BLOCK, count_of_...  21.1 us
    dot_general x1, matrix products, on_device(): down_sum = jnp.dot(hidden, down_full, preferred_element_type=jnp.float32)  20.7 us
    convert_element_type x28, local copies, waits for them, and re-layouts, entering(): part[k].astype(own.dtype)  12.1 us
  transfers between devices with their start and end apart: 4, of which 4 were waited for; matrix products, arithmetic and copies ran while one was open for 0% of the time, Pallas kernels for 0%

commit v1 on v0

--- a/solution.py
+++ b/solution.py
@@ -220,7 +220,9 @@
         0,
     )
     middle = (stream_in.astype(jnp.float32) + mixed_sum).astype(jnp.bfloat16)
-    normed = lax.all_gather(row_norm(middle, norm_gain), "tp", axis=0, tiled=True)
+    value = row_norm(middle, norm_gain)
+    copies = jnp.concatenate([value] * lax.axis_size("tp"), axis=0)
+    normed = lax.all_to_all(copies, "tp", 0, 0, tiled=True)
     up_sum = jnp.dot(normed, up_full, preferred_element_type=jnp.float32)
     hidden = jnp.square(jax.nn.relu(up_sum)).astype(jnp.bfloat16)
     down_sum = jnp.dot(hidden, down_full, preferred_element_type=jnp.float32)

time: 400 us -> 301 us (0.75)
  waiting for transfers between devices: 216 us -> 77.4 us
  blocking collectives: 35.5 us -> 73.5 us
    all_gather x1, waiting for transfers between devices: 103 us -> 0.01 us  [rows_first(): out, at, finished = (lax.all_gather(both, axis, axis=0, tiled=True), 0, [])]
    all_gather x1 -> x0, waiting for transfers between devices: 47.7 us -> none  [on_device(): lax.all_gather(row_norm(middle, norm_gain), 'tp', axis=0, tiled=True)]
    all_to_all x0 -> x1, blocking collectives: none -> 33 us  [on_device(): normed = lax.all_to_all(copies, 'tp', 0, 0, tiled=True)]
    reduce_scatter x1, waiting for transfers between devices: 37.5 us -> 46.7 us  [on_device(): lax.psum_scatter(down_sum.astype(jnp.bfloat16), 'tp', scatter_dimension=0...]
    all_gather x3, blocking collectives: 35.5 us -> 40.4 us  [gathered_once(): both, at, found = (lax.all_gather(jnp.concatenate(lines), axis), 0, {})]
  transfers between devices with their start and end apart: 4 -> 3, of which waited for: 4 -> 2; matrix products, arithmetic and copies ran while one was open for 0% -> 28% of each run, Pallas kernels for 0% -> 0%
where the time goes in v1:
time: 301 us; the launch traced here: 300 us
  waiting for transfers between devices  77.4 us (26%)
  blocking collectives  73.5 us (24%)
  local copies, waits for them, and re-layouts  52.8 us (18%)
  matrix products  36 us (12%)
  between operations  26.9 us (9%)
  other arithmetic  23.4 us (8%)
  starting transfers between devices  5.01 us (2%)
  loops' own time  4.82 us (2%)
    reduce_scatter x1, waiting for transfers between devices, on_device(): lax.psum_scatter(down_sum.astype(jnp.bfloat16), 'tp', scatter_dimension=0...  46.7 us
    all_gather x3, blocking collectives, gathered_once(): both, at, found = (lax.all_gather(jnp.concatenate(lines), axis), 0, {})  40.4 us
    all_to_all x1, blocking collectives, on_device(): normed = lax.all_to_all(copies, 'tp', 0, 0, tiled=True)  33 us
    all_to_all x1, waiting for transfers between devices, sum_at_owner(): lax.all_to_all(tiles, axis, split_axis=0, concat_axis=0, tiled=True)  30.6 us
    dynamic_update_slice x18, local copies, waits for them, and re-layouts, local_group(): lax.scan(block_step, carried, (query_rot.reshape(blocks, BLOCK, count_of_...  21.1 us
    dot_general x1, matrix products, on_device(): down_sum = jnp.dot(hidden, down_full, preferred_element_type=jnp.float32)  20.7 us
    convert_element_type x28, local copies, waits for them, and re-layouts, entering(): part[k].astype(own.dtype)  11 us
  transfers between devices with their start and end apart: 3, of which 2 were waited for; matrix products, arithmetic and copies ran while one was open for 28% of the time, Pallas kernels for 0%

profile of v1, /device:TPU:1, one launch (start us, length us, event | category | flops | bytes accessed | tf_op | source)
XLA Modules:
  0.0 299.9 jit_solution(14953674954953249489)
XLA Ops:
  6.5 1.7 pad_maximum_fusion.3
  8.4 1.1 copy.156
  9.5 1.1 copy.158
  12.2 25.0 %while.27 = (s32[]{:T(128)}, f32[2,64,64]{2,1,0:T(8,128)S(1)}, f32[6,128,2,64]{1,0,3,2:T(8,128)}, f32[6,128,2]{2,1,0:T(8,128)S(1)}, f32[6,128,2,64]{1,0,3,2:T(8,...) while((s32[]{:T(128)}, f32[2,64,64]{2,1,0:T(8,128)S(1)}, ...), condition=%wide.region_5.6_spmd.clone, body=%wide.region_3.5_spmd.clone.sunk | while | flops 12877827 | bytes 1099440 | solution.py:132
  13.3 2.8 dynamic_update_slice.14
  17.4 2.8 dynamic_update_slice.14
  21.6 2.8 dynamic_update_slice.14
  25.8 2.8 dynamic_update_slice.14
  29.9 2.8 dynamic_update_slice.14
  34.1 2.8 dynamic_update_slice.14
  37.2 1.0 reshape_reshape.22
  43.3 1.9 fusion.88
  45.4 0.9 maximum_multiply_fusion.1
  46.3 23.6 %while.26 = (s32[]{:T(128)}, f32[1,128,128]{2,1,0:T(8,128)S(1)}, f32[6,128,1,128]{3,1,0,2:T(8,128)}, f32[6,128,1]{1,2,0:T(1,128)S(1)}, f32[6,128,1,128]{3,2,1,0:...) while((s32[]{:T(128)}, f32[1,128,128]{2,1,0:T(8,128)S(1)}, ...), condition=%wide.region_2.3_spmd.clone, body=%wide.region_0.2_spmd.clone.sunk | while | flops 17006596 | bytes 1515172 | solution.py:132
  70.0 4.8 %all-gather.3 = bf16[2,194,128]{2,1,0:T(8,128)(2,1)S(1)} all-gather(bf16[1,194,128]{2,1,0:T(8,128)(2,1)S(1)} %maximum_bitcast_fusion), channel_id=2, replica_groups=mesh['sp_0'=8,'sp_1'=4,'sp_2'=2,'tp'=4] {'sp_2'}, dimensions={0}, use_global_device_ids=true | all-gather | bytes 148992 | tf_op jit(solution)/shard_map/all_gather | solution.py:42
  78.8 11.7 %all-gather.4 = bf16[4,194,128]{2,1,0:T(8,128)(2,1)S(1)} all-gather(bf16[1,194,128]{2,1,0:T(8,128)(2,1)S(1)} %maximum_bitcast_fusion.1), channel_id=3, replica_groups=mesh['sp_0'=8,'sp_1'=4,'sp_2'=2,'tp'=4] {'sp_1'}, dimensions={0}, use_global_device_ids=true | all-gather | bytes 248320 | tf_op jit(solution)/shard_map/all_gather | solution.py:42
  96.6 24.0 %all-gather.5 = bf16[8,194,128]{2,1,0:T(8,128)(2,1)S(1)} all-gather(bf16[1,194,128]{2,1,0:T(8,128)(2,1)S(1)} %maximum_bitcast_fusion.2), channel_id=4, replica_groups=mesh['sp_0'=8,'sp_1'=4,'sp_2'=2,'tp'=4] {'sp_0'}, dimensions={0}, use_global_device_ids=true | all-gather | bytes 446976 | tf_op jit(solution)/shard_map/all_gather | solution.py:42
  124.6 0.7 copy.178
  131.8 1.1 copy.170
  139.4 1.9 copy.169
  141.3 1.1 copy.153
  143.7 1.5 fusion.291
  145.3 1.5 fusion.292
  147.2 1.0 fusion.93
  148.2 2.7 add_convert_fusion
  150.9 4.8 %all-to-all-start = ((bf16[4,192,2048]{2,1,0:T(8,128)(2,1)}), bf16[4,192,2048]{2,1,0:T(8,128)(2,1)}, u32[]{:S(2)}, u32[]{:S(2)}) async-start(bf16[4,192,2048]{2,1,0:T(8,128)(2,1)} %bitcast.456), calls=%async_computation | async-start | bytes 6291456 | tf_op jit(solution)/shard_map/all_to_all | solution.py:82
  156.0 30.6 %all-to-all-done = bf16[4,192,2048]{2,1,0:T(8,128)(2,1)} async-done(((bf16[4,192,2048]{2,1,0:T(8,128)(2,1)}), bf16[4,192,2048]{2,1,0:T(8,128)(2,1)}, u32[]{:S(2)}, u32[]{:S(2)}) %all-to-all-start) | async-done | bytes 3145760 | tf_op jit(solution)/shard_map/all_to_all | solution.py:82
  186.6 2.6 convert_reduce_fusion
  190.3 33.0 %all_to_all.17 = bf16[4,192,2048]{2,1,0:T(8,128)(2,1)} all-to-all(bf16[4,192,2048]{2,1,0:T(8,128)(2,1)S(1)} %bitcast.457), channel_id=1, replica_groups=mesh['sp_0'=8,'sp_1'=4,'sp_2'=2,'tp'=4] {'tp'}, dimensions={0} | all-to-all | bytes 6291456 | tf_op jit(solution)/shard_map/all_to_all | solution.py:225
  223.3 20.7 %fusion.55 = bf16[768,2048]{1,0:T(8,128)(2,1)} fusion(bf16[2048,4096]{1,0:T(8,128)(2,1)} %all-gather.8.cloned.1.call-done, bf16[768,2048]{1,0:T(8,128)(2,1)} %bitcast.465), kind=kOutput, calls=%fused_computation.75 | convolution fusion | flops 12891193344 | bytes 23068672 | tf_op jit(solution)/shard_map/dot_general | solution.py:228
  244.1 46.7 %reduce-scatter.2.cloned.1.call-done = bf16[192,2048]{1,0:T(8,128)(2,1)} async-done(((bf16[768,2048]{1,0:T(8,128)(2,1)}), bf16[192,2048]{1,0:T(8,128)(2,1)}) %reduce-scatter.2.cloned.1.call-update) | async-done | bytes 786448 | tf_op jit(solution)/shard_map/reduce_scatter | solution.py:229
  290.8 2.2 fusion.64
  (331 shorter events, 51.0 us)
Async XLA Ops:
  6.5 140.6 %copy-start = (bf16[128,2048]{1,0:T(8,128)(2,1)S(1)}, bf16[128,2048]{1,0:T(8,128)(2,1)}, u32[]{:S(2)}) copy-start(bf16[128,2048]{1,0:T(8,128)(2,1)} %param.31) | copy-start | bytes 1572868
  6.5 216.8 %all-gather.8.cloned.1.call-start = ((), (), s32[]{:S(2)}) async-start(), calls=%async_computation.3 | async-start | bytes 17039360 | tf_op jit(solution)/shard_map/all_gather | solution.py:20
  8.3 3.0 copy-start.11
  9.5 2.4 copy-start.12
  12.1 26.1 %copy-start.19 = (f32[1,768]{1,0:T(1,128)S(1)}, f32[1,768]{1,0:T(1,128)}, u32[]{:S(2)}) copy-start(f32[1,768]{1,0:T(1,128)} %param.25) | copy-start | bytes 9220
  12.1 31.1 %copy-start.9 = (bf16[768,128]{1,0:T(8,128)(2,1)S(1)}, bf16[768,128]{1,0:T(8,128)(2,1)}, u32[]{:S(2)}) copy-start(bf16[768,128]{1,0:T(8,128)(2,1)} %param.21) | copy-start | bytes 589828
  12.1 31.1 %copy-start.10 = (bf16[768,128]{1,0:T(8,128)(2,1)S(1)}, bf16[768,128]{1,0:T(8,128)(2,1)}, u32[]{:S(2)}) copy-start(bf16[768,128]{1,0:T(8,128)(2,1)} %param.22) | copy-start | bytes 589828
  38.9 0.5 copy-start.21
  75.9 0.6 copy-start.14
  76.7 0.5 copy-start.20
  77.3 54.4 %copy-start.3 = (f32[6,128,2,64]{1,0,3,2:T(8,128)S(1)}, f32[6,128,2,64]{1,0,3,2:T(8,128)}, u32[]{:S(2)}) copy-start(f32[6,128,2,64]{1,0,3,2:T(8,128)} %get-tuple-element.84) | copy-start | bytes 1179652
  94.0 0.5 copy-start.13
  94.7 0.6 copy-start.15
  94.7 0.7 copy-start.17
  94.7 0.9 copy-start.16
  131.8 13.5 %copy-start.4 = (f32[2,64,64]{1,2,0:T(8,128)S(1)}, f32[2,64,64]{1,2,0:T(8,128)}, u32[]{:S(2)}) copy-start(f32[2,64,64]{1,2,0:T(8,128)} %copy.181) | copy-start | bytes 98308
  131.8 13.5 %copy-start.5 = (f32[2,64,64]{1,2,0:T(8,128)S(1)}, f32[2,64,64]{1,2,0:T(8,128)}, u32[]{:S(2)}) copy-start(f32[2,64,64]{1,2,0:T(8,128)} %copy.182) | copy-start | bytes 98308
  131.8 13.5 %copy-start.6 = (f32[2,64,64]{1,2,0:T(8,128)S(1)}, f32[2,64,64]{1,2,0:T(8,128)}, u32[]{:S(2)}) copy-start(f32[2,64,64]{1,2,0:T(8,128)} %copy.183) | copy-start | bytes 98308
  131.8 13.5 %copy-start.7 = (f32[2,64,64]{1,2,0:T(8,128)S(1)}, f32[2,64,64]{1,2,0:T(8,128)}, u32[]{:S(2)}) copy-start(f32[2,64,64]{1,2,0:T(8,128)} %copy.184) | copy-start | bytes 98308
  131.8 13.5 %copy-start.8 = (f32[2,64,64]{1,2,0:T(8,128)S(1)}, f32[2,64,64]{1,2,0:T(8,128)}, u32[]{:S(2)}) copy-start(f32[2,64,64]{1,2,0:T(8,128)} %copy.185) | copy-start | bytes 98308
  147.2 1.1 copy-start.2
  150.9 5.0 %copy-start.18 = (bf16[2048]{0:T(1024)(128)(2,1)S(1)}, bf16[2048]{0:T(1024)(128)(2,1)}, u32[]{:S(2)}) copy-start(bf16[2048]{0:T(1024)(128)(2,1)} %param.33) | copy-start | bytes 12292
  150.9 35.7 %all-to-all-start = ((bf16[4,192,2048]{2,1,0:T(8,128)(2,1)}), bf16[4,192,2048]{2,1,0:T(8,128)(2,1)}, u32[]{:S(2)}, u32[]{:S(2)}) async-start(bf16[4,192,2048]{2,1,0:T(8,128)(2,1)} %bitcast.456), calls=%async_computation | async-start | bytes 6291456 | tf_op jit(solution)/shard_map/all_to_all | solution.py:82
  155.7 33.5 %copy-start.1 = (bf16[192,2048]{1,0:T(8,128)(2,1)S(1)}, bf16[192,2048]{1,0:T(8,128)(2,1)}, u32[]{:S(2)}) copy-start(bf16[192,2048]{1,0:T(8,128)(2,1)} %param.20) | copy-start | bytes 2359300
  155.7 135.1 %reduce-scatter.2.cloned.1.call-start = ((), (), s32[]{:S(2)}) async-start(), calls=%async_computation.4 | async-start | bytes 3932160 | tf_op jit(solution)/shard_map/reduce_scatter | solution.py:229
Sparse Core Ops, SparseCore 0:
  10.1 107.1 all-gather.7
  244.2 46.5 reduce-scatter.1
